TPU v7x, 32 devices: a whole 2x2x4 slice. The times are simulated.
32 devices in a mesh: sp: 16 (over z, y, x), tp: 2 (over core).
Axes of the slice: x: 2, y: 2, z: 4, core: 2. Of those that a mesh axis runs over, the one named last changes fastest.
Arguments:
- queries: bfloat16 [4096, 1024], P('sp', 'tp'), may hold values from -6 to 6
- keys: bfloat16 [4096, 256], P('sp'), may hold values from -6 to 6
- values: bfloat16 [4096, 256], P('sp'), may hold values from -6 to 6
- query_gain: float32 [128], replicated, may hold values from 1.4 to 5.5
- key_gain: float32 [128], replicated, may hold values from 1.4 to 5.5
- residual_in: bfloat16 [4096, 2048], P(('sp', 'tp')), may hold values from -6 to 6
- out_weight: bfloat16 [1024, 2048], P('tp'), may hold values from -0.1875 to 0.1875
- norm_gain: float32 [2048], replicated, may hold values from 0.1 to 1.9
- gate_weight: bfloat16 [2048, 3072], P('sp', 'tp'), may hold values from -0.125 to 0.125
- up_weight: bfloat16 [2048, 3072], P('sp', 'tp'), may hold values from -0.125 to 0.125
- down_weight: bfloat16 [3072, 2048], P('tp', 'sp'), may hold values from -0.109375 to 0.109375
Outputs:
- result: bfloat16 [4096, 2048], P(('sp', 'tp'))
All inputs are finite; a program needn't handle non-finite values.
Results may differ from a plain program's by a relative error of at most 0.017.
Values may be sent and summed in bfloat16 or wider, within the bound.
A program may use at most 64 MiB of HBM per device.

v0:
```python
import math

import jax
import jax.numpy as jnp
from jax import lax
from jax.sharding import PartitionSpec as P

Q_HEADS = 8
KV_HEADS = 2
GRID_WIDTH = 64


EPS = 1e-06
ROPE_BASE = 10000.0


def normalize(wide_values, gain):
    wide = wide_values.astype(jnp.float32)
    return wide * lax.rsqrt(jnp.mean(wide * wide, axis=-1, keepdims=True) + EPS) * gain


def rotate_pair(segment, angles):
    half_size = segment.shape[-1] // 2
    first = segment[..., :half_size]
    second = segment[..., half_size:]
    cosine = jnp.cos(angles)[:, None, :]
    sine_part = jnp.sin(angles)[:, None, :]
    return jnp.concatenate(
        [first * cosine - second * sine_part, second * cosine + first * sine_part], axis=-1
    )


def grid_rotary(head_rows, positions):
    head_size = head_rows.shape[-1]
    half_size = head_size // 2
    quarter = head_size // 4
    inverse = ROPE_BASE ** (-jnp.arange(quarter, dtype=jnp.float32) * 2.0 / half_size)
    row_angles = (positions // GRID_WIDTH).astype(jnp.float32)[:, None] * inverse
    col_angles = (positions % GRID_WIDTH).astype(jnp.float32)[:, None] * inverse
    return jnp.concatenate(
        [
            rotate_pair(head_rows[..., :half_size], row_angles),
            rotate_pair(head_rows[..., half_size:], col_angles),
        ],
        axis=-1,
    )


def gated(gate_part, lifted):
    return (jax.nn.silu(gate_part) * lifted).astype(jnp.bfloat16)


def local(
    queries,
    keys,
    values,
    query_gain,
    key_gain,
    residual_in,
    out_weight,
    norm_gain,
    gate_weight,
    up_weight,
    down_weight,
):
    tok_rows = queries.shape[0]
    head_size = query_gain.shape[0]
    local_heads = queries.shape[1] // head_size
    tp_index = lax.axis_index("tp")
    share = tok_rows // lax.axis_size("tp")
    positions = lax.axis_index("sp") * tok_rows + jnp.arange(tok_rows, dtype=jnp.int32)
    key_head = tp_index * local_heads // (Q_HEADS // KV_HEADS)
    own_keys = lax.dynamic_slice_in_dim(keys, key_head * head_size, head_size, 1)
    own_values = lax.dynamic_slice_in_dim(values, key_head * head_size, head_size, 1)
    turned_keys = grid_rotary(
        normalize(own_keys.reshape(tok_rows, 1, head_size), key_gain), positions
    )
    turned_keys = turned_keys.reshape(tok_rows, head_size).astype(jnp.bfloat16)
    turned_queries = grid_rotary(
        normalize(queries.reshape(tok_rows, local_heads, head_size), query_gain), positions
    )
    turned_queries = turned_queries.reshape(tok_rows * local_heads, head_size).astype(jnp.bfloat16)
    score_scale = head_size ** (-0.5)

    def attend_block(running, block_pair):
        peak_score, weight_total, weighted = running
        block_keys, block_values = block_pair
        scores = (
            lax.dot_general(
                turned_queries,
                block_keys,
                (((1,), (1,)), ((), ())),
                preferred_element_type=jnp.float32,
            )
            * score_scale
        )
        new_peak = jnp.maximum(peak_score, jnp.max(scores, axis=1))
        factor = jnp.exp(peak_score - new_peak)
        raw = jnp.exp(scores - new_peak[:, None])
        weight_total = weight_total * factor + jnp.sum(raw, axis=1)
        weighted = weighted * factor[:, None] + jnp.dot(
            raw.astype(jnp.bfloat16), block_values, preferred_element_type=jnp.float32
        )
        return ((new_peak, weight_total, weighted), None)

    row_count = tok_rows * local_heads
    start_carry = (
        jnp.full((row_count,), -1e30, jnp.float32),
        jnp.zeros((row_count,), jnp.float32),
        jnp.zeros((row_count, head_size), jnp.float32),
    )
    piece_keys = lax.all_gather(turned_keys, "sp", axis=0, tiled=True)
    piece_values = lax.all_gather(own_values, "sp", axis=0, tiled=True)
    span = math.gcd(piece_keys.shape[0], 512)
    blocks = piece_keys.shape[0] // span
    stacked = (
        piece_keys.reshape(blocks, span, head_size),
        piece_values.reshape(blocks, span, head_size),
    )
    updated, unused = lax.scan(attend_block, start_carry, stacked)
    peak_score, weight_total, weighted = updated
    attended = (
        (weighted / weight_total[:, None])
        .astype(jnp.bfloat16)
        .reshape(tok_rows, local_heads * head_size)
    )
    placed = lax.dynamic_update_slice_in_dim(
        jnp.zeros((tok_rows, residual_in.shape[1]), jnp.float32),
        residual_in.astype(jnp.float32),
        tp_index * share,
        0,
    )
    head_partial = jnp.dot(attended, out_weight, preferred_element_type=jnp.float32)
    partial_total, residual_rows = (
        lax.psum(head_partial.astype(jnp.bfloat16), "tp").astype(jnp.float32),
        lax.psum(placed.astype(jnp.bfloat16), "tp").astype(jnp.float32),
    )
    middle_rows = (residual_rows + partial_total).astype(jnp.bfloat16)
    normed = normalize(middle_rows, norm_gain).astype(jnp.bfloat16)
    middle = lax.dynamic_slice_in_dim(middle_rows, tp_index * share, share, 0)
    hidden_width = gate_weight.shape[1]
    side_by_side = jnp.concatenate(
        [
            lax.all_gather(gate_weight, "sp", axis=0, tiled=True),
            lax.all_gather(up_weight, "sp", axis=0, tiled=True),
        ],
        axis=1,
    )
    both_parts = jnp.dot(normed, side_by_side, preferred_element_type=jnp.float32)
    hidden = gated(both_parts[:, :hidden_width], both_parts[:, hidden_width:])
    partials = jnp.dot(
        hidden,
        lax.all_gather(down_weight, "sp", axis=1, tiled=True),
        preferred_element_type=jnp.float32,
    )
    mixer_out = lax.psum_scatter(
        partials.astype(jnp.bfloat16), "tp", scatter_dimension=0, tiled=True
    ).astype(jnp.float32)
    return (middle.astype(jnp.float32) + mixer_out).astype(jnp.bfloat16)


def solution(mesh):
    return jax.shard_map(
        local,
        mesh=mesh,
        in_specs=(
            P("sp", "tp"),
            P("sp", None),
            P("sp", None),
            P(),
            P(),
            P(("sp", "tp"), None),
            P("tp", None),
            P(),
            P("sp", "tp"),
            P("sp", "tp"),
            P("tp", "sp"),
        ),
        out_specs=P(("sp", "tp"), None),
        check_vma=False,
    )
```

profile of v0, /device:TPU:0, one launch (start us, length us, event | category | flops | bytes accessed | tf_op | source)
XLA Modules:
  0.0 528.7 jit_solution(11063251506600256293)
XLA Ops:
  6.6 1.0 constant_dynamic-slice_fusion.1
  7.6 0.1 copy.20
  7.7 0.7 fusion.29
  8.5 0.3 fusion.43
  8.8 0.6 pad_maximum_fusion.1
  9.5 1.5 constant_dynamic-slice_fusion
  11.1 1.1 reshape.287
  12.2 0.3 multiply_reduce_fusion.1
  12.6 1.0 multiply_cosine_fusion.1
  13.6 0.3 multiply_multiply_fusion
  13.9 0.9 subtract_convert_fusion.1
  14.9 0.8 pad_maximum_fusion
  15.7 1.1 broadcast_in_dim.8
  16.8 0.9 convert_dynamic-update-slice_fusion
  17.7 50.1 %all-gather.15.cloned.1.call-done = bf16[4096,1,128]{0,2,1:T(8,128)(2,1)} async-done(((bf16[256,1,128]{0,2,1:T(8,128)(2,1)}), bf16[4096,1,128]{0,2,1:T(8,128)(2,1)}) %all-gather.15.cloned.1.call-update) | async-done | bytes 1048592 | tf_op jit(solution)/shard_map/all_gather | solution.py:112
  67.8 2.3 copy.19
  70.1 54.3 %all-gather.7.cloned.1.call-done = bf16[4096,128]{1,0:T(8,128)(2,1)} async-done(((bf16[256,128]{1,0:T(8,128)(2,1)}), bf16[4096,128]{1,0:T(8,128)(2,1)}) %all-gather.7.cloned.1.call-update) | async-done | bytes 1048592 | tf_op jit(solution)/shard_map/all_gather | solution.py:113
  124.4 51.7 %while.15 = (s32[]{:T(128)}, f32[1024]{0:T(1024)S(1)}, f32[1024]{0:T(1024)S(1)}, f32[1024,128]{1,0:T(8,128)S(1)}, bf16[8,512,128]{2,1,0:T(8,128)(2,1)}, /*index=...) while((s32[]{:T(128)}, f32[1024]{0:T(1024)S(1)}, ...), condition=%wide.region_6.7_spmd.clone, body=%wide.region_3.6_spmd.clone.sunk | while | flops 273028096 | bytes 16319621 | solution.py:120
  124.4 2.7 multiply_reduce_fusion.3
  127.0 2.1 fusion.63
  129.2 0.1 copy-done.1
  129.3 1.5 convolution_add_fusion.2
  130.8 2.7 multiply_reduce_fusion.3
  133.5 2.1 fusion.63
  135.6 0.1 copy-done.1
  135.7 1.5 convolution_add_fusion.2
  137.3 2.7 multiply_reduce_fusion.3
  140.0 2.1 fusion.63
  142.1 0.1 copy-done.1
  142.2 1.5 convolution_add_fusion.2
  143.7 2.7 multiply_reduce_fusion.3
  146.4 2.1 fusion.63
  148.5 0.1 copy-done.1
  148.6 1.5 convolution_add_fusion.2
  150.2 2.7 multiply_reduce_fusion.3
  152.9 2.1 fusion.63
  155.0 0.1 copy-done.1
  155.1 1.5 convolution_add_fusion.2
  156.7 2.7 multiply_reduce_fusion.3
  159.3 2.1 fusion.63
  161.5 0.1 copy-done.1
  161.6 1.5 convolution_add_fusion.2
  163.1 2.7 multiply_reduce_fusion.3
  165.8 2.1 fusion.63
  167.9 0.1 copy-done.1
  168.0 1.5 convolution_add_fusion.2
  169.6 2.7 multiply_reduce_fusion.3
  172.3 2.1 fusion.63
  174.5 1.5 convolution_add_fusion.2
  176.0 0.2 divide_convert_fusion
  176.2 0.2 reshape.286
  176.4 1.7 convolution_convert_fusion
  178.2 0.5 all-gather.11.cloned.1.call-update
  178.8 0.5 all-gather.9.cloned.1.call-update
  179.4 0.5 all-gather.13.cloned.1.call-update
  179.9 18.6 %all-reduce.3.cloned.1.call-done = (bf16[256,2048]{1,0:T(8,128)(2,1)}, bf16[256,2048]{1,0:T(8,128)(2,1)}) async-done(((bf16[256,2048]{1,0:T(8,128)(2,1)}, bf16[256,2048]{1,0:T(8,128)(2,1)}), (bf16[256,2048]{1,0:T(8,128)(2,1)}, bf16[256,2048]{1,0:T(8,128)(2,1)})) %all-reduce.3.cloned.1.call-update) | async-done | bytes 2097168 | tf_op jit(solution)/shard_map/psum | solution.py:135
  198.5 2.0 fusion.18
  200.6 95.2 %all-gather.11.cloned.1.call-done = bf16[2048,1536]{1,0:T(8,128)(2,1)} async-done(((bf16[128,1536]{1,0:T(8,128)(2,1)}), bf16[2048,1536]{1,0:T(8,128)(2,1)}) %all-gather.11.cloned.1.call-update) | async-done | bytes 6291472 | tf_op jit(solution)/shard_map/all_gather | solution.py:145
  295.8 94.6 %all-gather.9.cloned.1.call-done = bf16[2048,1536]{1,0:T(8,128)(2,1)} async-done(((bf16[128,1536]{1,0:T(8,128)(2,1)}), bf16[2048,1536]{1,0:T(8,128)(2,1)}) %all-gather.9.cloned.1.call-update) | async-done | bytes 6291472 | tf_op jit(solution)/shard_map/all_gather | solution.py:144
  390.4 9.8 %fusion.14 = f32[256,3072]{1,0:T(8,128)} fusion(bf16[2048,1536]{1,0:T(8,128)(2,1)} %all-gather.11.cloned.1.call-done, bf16[2048,1536]{1,0:T(8,128)(2,1)} %all-gather.9.cloned.1.call-done, bf16[256,2048]{1,0:T(8,128)(2,1)S(1)} %get-tuple-element.102, f32[2048]{0:T(1024)S(1)} %copy-done.4, f32[256]{0:T(256)S(1)} %add_rsqrt_fusion.1), kind=kOutput, calls=%fused_computation.20 | convolution fusion | flops 3248488448 | bytes 16786432 | tf_op jit(solution)/shard_map/dot_general | solution.py:149
  400.2 106.3 %all-gather.13.cloned.1.call-done = bf16[1536,2048]{1,0:T(8,128)(2,1)} async-done(((bf16[1536,128]{1,0:T(8,128)(2,1)}), bf16[1536,2048]{1,0:T(8,128)(2,1)}) %all-gather.13.cloned.1.call-update) | async-done | bytes 6291472 | tf_op jit(solution)/shard_map/all_gather | solution.py:153
  506.5 6.6 %convolution_convert_fusion.1 = bf16[256,2048]{1,0:T(8,128)(2,1)} fusion(bf16[1536,2048]{1,0:T(8,128)(2,1)} %all-gather.13.cloned.1.call-done, f32[256,3072]{1,0:T(8,128)} %fusion.14), kind=kOutput, calls=%fused_computation.27 | convolution fusion | flops 1613496320 | bytes 10485760 | tf_op jit(solution)/shard_map/dot_general | solution.py:151
  513.1 6.7 %reduce-scatter.2.cloned.1.call-done = bf16[128,2048]{1,0:T(8,128)(2,1)} async-done(((bf16[256,2048]{1,0:T(8,128)(2,1)}), bf16[128,2048]{1,0:T(8,128)(2,1)}) %reduce-scatter.2.cloned.1.call-update) | async-done | bytes 524304 | tf_op jit(solution)/shard_map/reduce_scatter | solution.py:156
  519.9 2.0 add_convert_fusion.1
  (61 shorter events, 0.7 us)
Async XLA Ops:
  6.5 169.9 %copy-start = (bf16[512,2048]{1,0:T(8,128)(2,1)S(1)}, bf16[512,2048]{1,0:T(8,128)(2,1)}, u32[]{:S(2)}) copy-start(bf16[512,2048]{1,0:T(8,128)(2,1)} %param.19) | copy-start | bytes 6291460
  6.5 7.1 %copy-start.3 = (f32[128]{0:T(128)S(1)}, f32[128]{0:T(128)}, u32[]{:S(2)}) copy-start(f32[128]{0:T(128)} %param.16) | copy-start | bytes 1540
  6.5 61.3 %all-gather.15.cloned.1.call-start = ((), (), s32[]{:S(2)}) async-start(), calls=%async_computation.6 | async-start | bytes 1114112 | tf_op jit(solution)/shard_map/all_gather | solution.py:112
  9.5 114.9 %all-gather.7.cloned.1.call-start = ((), (), s32[]{:S(2)}) async-start(), calls=%async_computation.1 | async-start | bytes 1114112 | tf_op jit(solution)/shard_map/all_gather | solution.py:113
  11.0 187.5 %all-reduce.3.cloned.1.call-start = ((), (), s32[]{:S(2)}) async-start(), calls=%async_computation.7 | async-start | bytes 4194304 | tf_op jit(solution)/shard_map/psum | solution.py:135
  14.8 2.0 copy-start.2
  127.0 2.2 copy-start.1
  133.5 2.2 copy-start.1
  140.0 2.2 copy-start.1
  146.4 2.2 copy-start.1
  152.9 2.2 copy-start.1
  159.3 2.2 copy-start.1
  165.8 2.2 copy-start.1
  172.3 2.2 copy-start.1
  178.1 212.2 %copy-start.4 = (f32[2048]{0:T(1024)S(1)}, f32[2048]{0:T(1024)}, u32[]{:S(2)}) copy-start(f32[2048]{0:T(1024)} %param.20) | copy-start | bytes 24580
  178.1 117.6 %all-gather.11.cloned.1.call-start = ((), (), s32[]{:S(2)}) async-start(), calls=%async_computation.3 | async-start | bytes 6684672 | tf_op jit(solution)/shard_map/all_gather | solution.py:145
  178.7 211.6 %all-gather.9.cloned.1.call-start = ((), (), s32[]{:S(2)}) async-start(), calls=%async_computation.2 | async-start | bytes 6684672 | tf_op jit(solution)/shard_map/all_gather | solution.py:144
  179.3 327.2 %all-gather.13.cloned.1.call-start = ((), (), s32[]{:S(2)}) async-start(), calls=%async_computation.4 | async-start | bytes 6684672 | tf_op jit(solution)/shard_map/all_gather | solution.py:153
  179.9 340.0 %reduce-scatter.2.cloned.1.call-start = ((), (), s32[]{:S(2)}) async-start(), calls=%async_computation.5 | async-start | bytes 1572864 | tf_op jit(solution)/shard_map/reduce_scatter | solution.py:156
Sparse Core Ops, SparseCore 0:
  10.1 57.6 all-gather.14
  70.6 53.7 all-gather.6
  178.3 20.2 all-reduce.2
  201.1 94.5 all-gather.10
  298.4 91.9 all-gather.8
  392.9 113.5 all-gather.12
  513.2 6.5 reduce-scatter.1
where the time goes:
time: 529 us
  waiting for transfers between devices  428 us (81%)
  matrix products  51.7 us (10%)
  other arithmetic  27.3 us (5%)
  between operations  13.7 us (3%)
  local copies, waits for them, and re-layouts  8.01 us (2%)
    all_gather x1, waiting for transfers between devices, local(): lax.all_gather(down_weight, 'sp', axis=1, tiled=True)  106 us
    all_gather x1, waiting for transfers between devices, local(): lax.all_gather(up_weight, 'sp', axis=0, tiled=True)  95.2 us
    all_gather x1, waiting for transfers between devices, local(): lax.all_gather(gate_weight, 'sp', axis=0, tiled=True)  94.6 us
    all_gather x1, waiting for transfers between devices, local(): piece_values = lax.all_gather(own_values, 'sp', axis=0, tiled=True)  54.3 us
    all_gather x1, waiting for transfers between devices, local(): piece_keys = lax.all_gather(turned_keys, 'sp', axis=0, tiled=True)  50.1 us
    dot_general x8, matrix products, attend_block(): lax.dot_general(turned_queries, block_keys, (((1,), (1,)), ((), ())), pre...  21.4 us
    psum x1, waiting for transfers between devices, local(): lax.psum(head_partial.astype(jnp.bfloat16), 'tp').astype(jnp.float32)  18.6 us
    reduce_sum x8, other arithmetic, attend_block(): weight_total = weight_total * factor + jnp.sum(raw, axis=1)  16.9 us
  transfers between devices with their start and end apart: 7, of which 7 were waited for; matrix products, arithmetic and copies ran while one was open for 4% of the time, Pallas kernels for 0%

commit v1 on v0

--- a/solution.py
+++ b/solution.py
@@ -1,8 +1,11 @@
+import functools
 import math
 
 import jax
 import jax.numpy as jnp
 from jax import lax
+from jax.experimental import pallas as pl
+from jax.experimental.pallas import tpu as pltpu
 from jax.sharding import PartitionSpec as P
 
 Q_HEADS = 8
@@ -159,9 +162,487 @@
     return (middle.astype(jnp.float32) + mixer_out).astype(jnp.bfloat16)
 
 
+MESH = pl.DeviceIdType.MESH
+MEMBERS = 4
+LOG2E = 1.4426950408889634
+
+
+def rotary_tables(tok_rows, head_size):
+    positions = lax.axis_index("sp") * tok_rows + jnp.arange(tok_rows, dtype=jnp.int32)
+    quarter = head_size // 4
+    lane = jnp.arange(head_size)
+    inverse = ROPE_BASE ** (-(lane % quarter).astype(jnp.float32) * 4.0 / head_size)
+    row = (positions // GRID_WIDTH).astype(jnp.float32)[:, None]
+    col = (positions % GRID_WIDTH).astype(jnp.float32)[:, None]
+    angles = jnp.where(lane[None, :] < head_size // 2, row, col) * inverse[None, :]
+    sign = jnp.where((lane // quarter) % 2 == 0, -1.0, 1.0)
+    return jnp.cos(angles), jnp.sin(angles) * sign[None, :]
+
+
+def layer_kernel(
+    n_sp,
+    queries,
+    keys,
+    values,
+    query_gain,
+    key_gain,
+    residual_in,
+    out_weight,
+    norm_gain,
+    gate_weight,
+    up_weight,
+    down_weight,
+    cosine,
+    sine,
+    result,
+    turned_q,
+    key_buf,
+    value_buf,
+    peak,
+    total,
+    weighted,
+    attended,
+    head_send,
+    head_own,
+    head_recv,
+    middle,
+    tokens,
+    gate_up,
+    down,
+    half_send,
+    half_recv,
+    share_send,
+    share_recv,
+    kv_send,
+    kv_recv,
+    w_send,
+    w_recv,
+    wf_send,
+    wf_recv,
+    h_send,
+    h_recv,
+    t_send,
+    t_recv,
+    o_send,
+    o_recv,
+):
+    f32, bf16 = jnp.float32, jnp.bfloat16
+    planes = n_sp // 4
+    s = lax.axis_index("sp")
+    t = lax.axis_index("tp")
+    hi, mid, lo = s // 4, (s // 2) % 2, s % 2
+    tok_rows, width = queries.shape
+    head_size = query_gain.shape[1]
+    heads = width // head_size
+    share = residual_in.shape[0]
+    model = residual_in.shape[1]
+    depth = gate_weight.shape[0]
+    part = gate_weight.shape[1] // MEMBERS
+    sibling = {"sp": s, "tp": 1 - t}
+
+    def at(hi_, mid_, lo_):
+        return hi_ * 4 + mid_ * 2 + lo_
+
+    def dev(sp_index):
+        return {"sp": sp_index, "tp": t}
+
+    x_peer = at(hi, mid, 1 - lo)
+    y_peer = at(hi, 1 - mid, lo)
+
+    def plane_peer(i):
+        return at((hi + i % planes) % planes, mid, (lo + i // planes) % 2)
+
+    def source_peer(i):
+        return at((hi + planes - i % planes) % planes, mid, (lo + i // planes) % 2)
+
+    def member(r):
+        return at(hi - hi % 2 + (hi % 2 + r // 2) % 2, mid, (lo + r % 2) % 2)
+
+    def remote(src, dst, ssem, rsem, device):
+        return pltpu.make_async_remote_copy(
+            src_ref=src, dst_ref=dst, send_sem=ssem, recv_sem=rsem,
+            device_id=device, device_id_type=MESH,
+        )
+
+    barrier = pltpu.get_barrier_semaphore()
+    for i in range(1, 2 * planes):
+        pl.semaphore_signal(barrier, inc=1, device_id=dev(plane_peer(i)), device_id_type=MESH)
+    pl.semaphore_signal(barrier, inc=1, device_id=dev(y_peer), device_id_type=MESH)
+    pl.semaphore_signal(barrier, inc=1, device_id=sibling, device_id_type=MESH)
+
+    quarter = head_size // 4
+    lanes = lax.broadcasted_iota(jnp.int32, (tok_rows, head_size), 1)
+    low_half = (lanes // quarter) % 2 == 0
+
+    def turn(rows, gain):
+        wide = rows.astype(f32)
+        wide = wide * lax.rsqrt(jnp.mean(wide * wide, axis=-1, keepdims=True) + EPS) * gain
+        partner = jnp.where(
+            low_half, pltpu.roll(wide, head_size - quarter, 1), pltpu.roll(wide, quarter, 1)
+        )
+        return (wide * cosine[...] + partner * sine[...]).astype(bf16)
+
+    key_head = (t * heads) // (Q_HEADS // KV_HEADS)
+    kv_cols = pl.ds(pl.multiple_of(key_head * head_size, head_size), head_size)
+    key_buf[0] = turn(keys[:, kv_cols], key_gain[...])
+    value_buf[0] = values[:, kv_cols].astype(f32).T.astype(bf16)
+    pl.semaphore_wait(barrier, 2 * planes + 1)
+
+    def key_copy(src, dst, hop, device):
+        return remote(key_buf.at[src], key_buf.at[dst], kv_send.at[0, hop, src], kv_recv.at[0, dst], device)
+
+    def value_copy(src, dst, hop, device):
+        return remote(value_buf.at[src], value_buf.at[dst], kv_send.at[1, hop, src], kv_recv.at[1, dst], device)
+
+    def z_copies(d):
+        device = dev(at((hi + d) % planes, mid, lo))
+        return [key_copy_z(d, device), value_copy_z(d, device)]
+
+    def key_copy_z(d, device):
+        return remote(key_buf.at[0], key_buf.at[d], kv_send.at[0, 2, d], kv_recv.at[0, d], device)
+
+    def value_copy_z(d, device):
+        return remote(value_buf.at[0], value_buf.at[d], kv_send.at[1, 2, d], kv_recv.at[1, d], device)
+
+    def first_copies(d):
+        return [
+            key_copy(d, planes + d, 0, dev(x_peer)),
+            value_copy(d, 2 * planes + d, 1, dev(y_peer)),
+            key_copy(d, 2 * planes + d, 1, dev(y_peer)),
+            value_copy(d, planes + d, 0, dev(x_peer)),
+        ]
+
+    def second_copies(d):
+        return [
+            key_copy(planes + d, 3 * planes + d, 1, dev(y_peer)),
+            value_copy(2 * planes + d, 3 * planes + d, 0, dev(x_peer)),
+        ]
+
+    def member_of(sp_index):
+        return sp_index % 2 + 2 * ((sp_index // 4) % 2)
+
+    def weight_refs(sp_index):
+        rows = pl.ds(pl.multiple_of(sp_index * depth, depth), depth)
+        return [
+            gate_up.at[rows, pl.ds(0, part)],
+            gate_up.at[rows, pl.ds(part, part)],
+            down.at[:, rows],
+        ]
+
+    def own_refs(target):
+        cols = pl.ds(pl.multiple_of(member_of(target) * part, part), part)
+        return [gate_weight.at[:, cols], up_weight.at[:, cols], down_weight.at[cols, :]]
+
+    def weight_copies(i):
+        target = plane_peer(i)
+        return [
+            remote(a, b, w_send.at[k, i], w_recv.at[k, i], dev(target))
+            for k, (a, b) in enumerate(zip(own_refs(target), weight_refs(s)))
+        ]
+
+    def forward_copies(i):
+        source = source_peer(i)
+        return [
+            remote(a, a, wf_send.at[k, i], wf_recv.at[k, i], dev(y_peer))
+            for k, a in enumerate(weight_refs(source))
+        ]
+
+    def own_forward():
+        return [
+            remote(a, b, wf_send.at[k, 0], wf_recv.at[k, 0], dev(y_peer))
+            for k, (a, b) in enumerate(zip(own_refs(s), weight_refs(s)))
+        ]
+
+    def start(copies):
+        for copy in copies:
+            copy.start()
+
+    def wait_recv(copies):
+        for copy in copies:
+            copy.wait_recv()
+
+    def wait_send(copies):
+        for copy in copies:
+            copy.wait_send()
+
+    def relay_weights(i):
+        wait_recv(weight_copies(i))
+        start(forward_copies(i))
+
+    for d in range(1, planes):
+        start(z_copies(d))
+    start(first_copies(0))
+    for i in range(1, planes):
+        start(weight_copies(i))
+
+    for a, b in zip(own_refs(s), weight_refs(s)):
+        b[...] = a[...]
+    for h in range(heads):
+        turned_q[h] = turn(queries[:, h * head_size : (h + 1) * head_size], query_gain[...])
+    peak[...] = jnp.full(peak.shape, -1e30, f32)
+    total[...] = jnp.zeros(total.shape, f32)
+    weighted[...] = jnp.zeros(weighted.shape, f32)
+    exponent_scale = head_size ** (-0.5) * LOG2E
+
+    def attend(slot):
+        block_keys = key_buf[slot]
+        block_values = value_buf[slot]
+        for h in range(heads):
+            scores = lax.dot_general(
+                block_keys, turned_q[h], (((1,), (1,)), ((), ())), preferred_element_type=f32
+            )
+            old_peak = peak[h]
+            new_peak = jnp.maximum(old_peak, jnp.max(scores, axis=0, keepdims=True))
+            factor = jnp.exp2((old_peak - new_peak) * exponent_scale)
+            raw = jnp.exp2((scores - new_peak) * exponent_scale)
+            total[h] = total[h] * factor + jnp.sum(raw, axis=0, keepdims=True)
+            weighted[h] = weighted[h] * factor + jnp.dot(
+                block_values, raw.astype(bf16), preferred_element_type=f32
+            )
+            peak[h] = new_peak
+
+    def first_step(d, carry):
+        wait_recv(z_copies(d))
+        start(first_copies(d))
+        return carry
+
+    def second_step(d, carry):
+        wait_recv([first_copies(d)[0], first_copies(d)[1]])
+        start(second_copies(d))
+        return carry
+
+    def attend_step(slot, carry):
+        attend(slot)
+        return carry
+
+    attend(0)
+    lax.fori_loop(1, planes, first_step, 0)
+    lax.fori_loop(1, planes, attend_step, 0)
+    lax.fori_loop(0, planes, second_step, 0)
+    start(own_forward())
+    for i in range(planes, 2 * planes):
+        start(weight_copies(i))
+
+    def third_step(d, carry):
+        first_copies(d)[3].wait_recv()
+        attend(planes + d)
+        return carry
+
+    def fourth_step(d, carry):
+        first_copies(d)[2].wait_recv()
+        attend(2 * planes + d)
+        return carry
+
+    def fifth_step(d, carry):
+        wait_recv(second_copies(d))
+        attend(3 * planes + d)
+
+        @pl.when(d > 0)
+        def _():
+            relay_weights(d)
+
+        return carry
+
+    lax.fori_loop(0, planes, third_step, 0)
+    lax.fori_loop(0, planes, fourth_step, 0)
+    lax.fori_loop(0, planes, fifth_step, 0)
+    for h in range(heads):
+        attended[:, h * head_size : (h + 1) * head_size] = (weighted[h] / total[h]).T.astype(bf16)
+
+    own_rows = pl.ds(pl.multiple_of(t * share, share), share)
+    other_rows = pl.ds(pl.multiple_of((1 - t) * share, share), share)
+    head_send[...] = jnp.dot(
+        attended[other_rows, :], out_weight[...], preferred_element_type=f32
+    ).astype(bf16)
+    head_copy = remote(head_send, head_recv, h_send, h_recv, sibling)
+    head_copy.start()
+    head_own[...] = jnp.dot(
+        attended[own_rows, :], out_weight[...], preferred_element_type=f32
+    ).astype(bf16)
+    head_copy.wait_recv()
+    added = head_own[...].astype(f32) + head_recv[...].astype(f32)
+    middle[...] = (residual_in[...].astype(f32) + added).astype(bf16)
+    wide = middle[...].astype(f32)
+    tokens[0, t] = (
+        wide * lax.rsqrt(jnp.mean(wide * wide, axis=-1, keepdims=True) + EPS) * norm_gain[...]
+    ).astype(bf16)
+
+    def token_copy(r):
+        return remote(
+            tokens.at[0, t], tokens.at[r, t], t_send.at[0, r], t_recv.at[0, r], dev(member(r))
+        )
+
+    def sibling_copy(r):
+        return remote(
+            tokens.at[r, t], tokens.at[r, t], t_send.at[1, r], t_recv.at[1, r], sibling
+        )
+
+    def sibling_arrival(r):
+        return remote(
+            tokens.at[r, 1 - t], tokens.at[r, 1 - t], t_send.at[1, r], t_recv.at[1, r], sibling
+        )
+
+    for r in range(1, MEMBERS):
+        token_copy(r).start()
+    sibling_copy(0).start()
+
+    def relay_step(i, carry):
+        relay_weights(i)
+        return carry
+
+    lax.fori_loop(planes, 2 * planes, relay_step, 0)
+    for r in range(1, MEMBERS):
+        token_copy(r).wait_recv()
+        sibling_copy(r).start()
+
+    def arrive_step(i, carry):
+        wait_recv(
+            [
+                remote(a, a, wf_send.at[k, i], wf_recv.at[k, i], dev(y_peer))
+                for k, a in enumerate(weight_refs(source_peer(i) + 2 - 4 * mid))
+            ]
+        )
+        return carry
+
+    lax.fori_loop(0, 2 * planes, arrive_step, 0)
+
+    def half_copy(r):
+        return remote(
+            half_send.at[r], half_recv.at[r], o_send.at[0, r], o_recv.at[0, r], sibling
+        )
+
+    def share_copy(r):
+        return remote(
+            share_send.at[r], share_recv.at[r], o_send.at[1, r], o_recv.at[1, r], dev(member(r))
+        )
+
+    def mix_step(step, carry):
+        r = (step + 1) % MEMBERS
+        sibling_arrival(r).wait_recv()
+        rows = tokens[r].reshape(2 * share, model)
+        both = jnp.dot(rows, gate_up[...], preferred_element_type=f32)
+        hidden = gated(both[:, :part], both[:, part:])
+        attended[:, 0:part] = hidden
+        half_send[r] = jnp.dot(
+            attended[other_rows, 0:part], down[...], preferred_element_type=f32
+        ).astype(bf16)
+        half_copy(r).start()
+        partial = jnp.dot(attended[own_rows, 0:part], down[...], preferred_element_type=f32)
+        half_copy(r).wait_recv()
+        share_send[r] = (partial + half_recv[r].astype(f32)).astype(bf16)
+
+        @pl.when(r > 0)
+        def _():
+            share_copy(r).start()
+
+        return carry
+
+    lax.fori_loop(0, MEMBERS, mix_step, 0)
+    out = middle[...].astype(f32) + share_send[0].astype(f32)
+    for r in range(1, MEMBERS):
+        share_copy(r).wait_recv()
+        out = out + share_recv[r].astype(f32)
+    result[...] = out.astype(bf16)
+
+    for d in range(1, planes):
+        wait_send(z_copies(d))
+    for d in range(planes):
+        wait_send(first_copies(d))
+        wait_send(second_copies(d))
+    wait_send(own_forward())
+    for i in range(1, 2 * planes):
+        wait_send(weight_copies(i))
+        wait_send(forward_copies(i))
+    head_copy.wait_send()
+    for r in range(MEMBERS):
+        sibling_copy(r).wait_send()
+        half_copy(r).wait_send()
+        if r > 0:
+            token_copy(r).wait_send()
+            share_copy(r).wait_send()
+
+
+def fused(
+    queries, keys, values, query_gain, key_gain, residual_in, out_weight, norm_gain,
+    gate_weight, up_weight, down_weight,
+):
+    n_sp = lax.axis_size("sp")
+    planes = n_sp // 4
+    tok_rows, width = queries.shape
+    head_size = query_gain.shape[0]
+    heads = width // head_size
+    share, model = residual_in.shape
+    part = gate_weight.shape[1] // MEMBERS
+    f32, bf16 = jnp.float32, jnp.bfloat16
+    cosine, sine = rotary_tables(tok_rows, head_size)
+    vmem = pl.BlockSpec(memory_space=pltpu.VMEM)
+    dma = pltpu.SemaphoreType.DMA
+    return pl.pallas_call(
+        functools.partial(layer_kernel, n_sp),
+        out_shape=jax.ShapeDtypeStruct((share, model), bf16),
+        in_specs=[vmem] * 13,
+        out_specs=vmem,
+        scratch_shapes=[
+            pltpu.VMEM((heads, tok_rows, head_size), bf16),
+            pltpu.VMEM((n_sp, tok_rows, head_size), bf16),
+            pltpu.VMEM((n_sp, head_size, tok_rows), bf16),
+            pltpu.VMEM((heads, 1, tok_rows), f32),
+            pltpu.VMEM((heads, 1, tok_rows), f32),
+            pltpu.VMEM((heads, head_size, tok_rows), f32),
+            pltpu.VMEM((tok_rows, max(width, part)), bf16),
+            pltpu.VMEM((share, model), bf16),
+            pltpu.VMEM((share, model), bf16),
+            pltpu.VMEM((share, model), bf16),
+            pltpu.VMEM((share, model), bf16),
+            pltpu.VMEM((MEMBERS, 2, share, model), bf16),
+            pltpu.VMEM((model, 2 * part), bf16),
+            pltpu.VMEM((part, model), bf16),
+            pltpu.VMEM((MEMBERS, share, model), bf16),
+            pltpu.VMEM((MEMBERS, share, model), bf16),
+            pltpu.VMEM((MEMBERS, share, model), bf16),
+            pltpu.VMEM((MEMBERS, share, model), bf16),
+            dma((2, 3, n_sp)),
+            dma((2, n_sp)),
+            dma((3, 2 * planes)),
+            dma((3, 2 * planes)),
+            dma((3, 2 * planes)),
+            dma((3, 2 * planes)),
+            dma,
+            dma,
+            dma((2, MEMBERS)),
+            dma((2, MEMBERS)),
+            dma((2, MEMBERS)),
+            dma((2, MEMBERS)),
+        ],
+        compiler_params=pltpu.CompilerParams(
+            collective_id=0, has_side_effects=True, vmem_limit_bytes=60 * 1024 * 1024
+        ),
+    )(
+        queries, keys, values, query_gain.reshape(1, -1), key_gain.reshape(1, -1), residual_in,
+        out_weight, norm_gain.reshape(1, -1), gate_weight, up_weight, down_weight, cosine, sine,
+    )
+
+
+def layer(*args):
+    queries, residual_in, gate_weight = args[0], args[5], args[8]
+    head_size = args[3].shape[0]
+    fits = (
+        lax.axis_size("sp") % 8 == 0
+        and lax.axis_size("tp") == 2
+        and residual_in.shape[0] * 2 == queries.shape[0]
+        and residual_in.shape[0] % 16 == 0
+        and head_size == 128
+        and queries.shape[1] % head_size == 0
+        and gate_weight.shape[0] % 128 == 0
+        and gate_weight.shape[1] % (128 * MEMBERS) == 0
+        and (Q_HEADS // KV_HEADS) % (queries.shape[1] // head_size) == 0
+    )
+    return fused(*args) if fits else local(*args)
+
+
 def solution(mesh):
     return jax.shard_map(
-        local,
+        layer,
         mesh=mesh,
         in_specs=(
             P("sp", "tp"),

time: 529 us -> 139 us (0.26)
  waiting for transfers between devices: 428 us -> 0 us
  Pallas kernels: 0 us -> 136 us
  matrix products: 51.7 us -> 0 us
  other arithmetic: 27.3 us -> 1.28 us
  between operations: 13.7 us -> 0.02 us
  local copies, waits for them, and re-layouts: 8.01 us -> 1.88 us
    all_gather x5 -> x0, waiting for transfers between devices: 401 us -> none  [the longest x1 106 us: local(): lax.all_gather(down_weight, 'sp', axis=1, tiled=True)]
    pallas_call x0 -> x1, Pallas kernels: none -> 136 us  [fused(): pl.pallas_call(functools.partial(layer_kernel, n_sp), out_shape=jax.Shape...]
    dot_general x19 -> x0, matrix products: 51.7 us -> none  [the longest x8 21.4 us: attend_block(): lax.dot_general(turned_queries, block_keys, (((1,), (1,)), ((), ())), pre...]
    reduce_sum x11 -> x0, other arithmetic: 19.3 us -> none  [the longest x8 16.9 us: attend_block(): weight_total = weight_total * factor + jnp.sum(raw, axis=1)]
    psum x1 -> x0, waiting for transfers between devices: 18.6 us -> none  [local(): lax.psum(head_partial.astype(jnp.bfloat16), 'tp').astype(jnp.float32)]
    reduce_scatter x1 -> x0, waiting for transfers between devices: 6.73 us -> none  [local(): lax.psum_scatter(partials.astype(jnp.bfloat16), 'tp', scatter_dimension=0...]
  transfers between devices with their start and end apart: 7 -> 0, of which waited for: 7 -> 0; matrix products, arithmetic and copies ran while one was open for 4% -> 0% of each run, Pallas kernels for 0% -> 0%
where the time goes in v1:
time: 139 us
  Pallas kernels  136 us (98%)
  local copies, waits for them, and re-layouts  1.88 us (1%)
    pallas_call x1, Pallas kernels, fused(): pl.pallas_call(functools.partial(layer_kernel, n_sp), out_shape=jax.Shape...  136 us

profile of v1, /device:TPU:0, one launch (start us, length us, event | category | flops | bytes accessed | tf_op | source)
XLA Modules:
  0.0 138.9 jit_solution(8238201301955836876)
XLA Ops:
  0.0 1.3 sine_multiply_fusion
  1.3 135.8 %shard_map.109 = bf16[128,2048]{1,0:T(8,128)(2,1)} custom-call(bf16[256,512]{1,0:T(8,128)(2,1)} %queries.1, bf16[256,256]{1,0:T(8,128)(2,1)} %keys.1, bf16[256,256]{1,0:T(8,128)(2,1)} %values.1, f32[1,128]{1,0:T(1,128)} %bitcast.4, f32[1,128]{1,0:T(1,128)} %bitcast.5, bf16[128,2048]{1,0:T(8,128)(2,1)} %residual_in.1, bf16[512,2048]{1,0:T(8,128)(2,1)} %out_weight.1, ...), custom_call_target="tpu_custom_call" | custom-call | tf_op jit(solution)/shard_map/pallas_call | solution.py:580
  137.1 1.9 %copy.13 = bf16[128,2048]{1,0:T(8,128)(2,1)} copy(bf16[128,2048]{1,0:T(8,128)(2,1)} %shard_map.109) | data formatting | bytes 1048576
  (3 shorter events, 0.0 us)

commit v2 on v1

--- a/solution.py
+++ b/solution.py
@@ -209,16 +209,21 @@
     tokens,
     gate_up,
     down,
+    stage_gate_up,
+    stage_down,
     half_send,
     half_recv,
     share_send,
     share_recv,
+    share_own,
     kv_send,
     kv_recv,
     w_send,
     w_recv,
     wf_send,
     wf_recv,
+    x_send,
+    x_recv,
     h_send,
     h_recv,
     t_send,
@@ -249,11 +254,14 @@
     x_peer = at(hi, mid, 1 - lo)
     y_peer = at(hi, 1 - mid, lo)
 
+    def plane(d, sign):
+        return (hi // 2 + planes + sign * (d // 2)) % (planes // 2) * 2 + (hi + d) % 2
+
     def plane_peer(i):
-        return at((hi + i % planes) % planes, mid, (lo + i // planes) % 2)
+        return at(plane(i % planes, 1), mid, (lo + i // planes) % 2)
 
     def source_peer(i):
-        return at((hi + planes - i % planes) % planes, mid, (lo + i // planes) % 2)
+        return at(plane(i % planes, -1), mid, (lo + i // planes) % 2)
 
     def member(r):
         return at(hi - hi % 2 + (hi % 2 + r // 2) % 2, mid, (lo + r % 2) % 2)
@@ -295,7 +303,7 @@
         return remote(value_buf.at[src], value_buf.at[dst], kv_send.at[1, hop, src], kv_recv.at[1, dst], device)
 
     def z_copies(d):
-        device = dev(at((hi + d) % planes, mid, lo))
+        device = dev(at(plane(d, 1), mid, lo))
         return [key_copy_z(d, device), value_copy_z(d, device)]
 
     def key_copy_z(d, device):
@@ -353,6 +361,32 @@
             for k, (a, b) in enumerate(zip(own_refs(s), weight_refs(s)))
         ]
 
+    def stage_refs(b):
+        return [
+            stage_gate_up.at[b, :, pl.ds(0, part)],
+            stage_gate_up.at[b, :, pl.ds(part, part)],
+            stage_down.at[b],
+        ]
+
+    def stage_copies(b):
+        return [
+            remote(a, c, x_send.at[k, b], x_recv.at[k, b], dev(x_peer))
+            for k, (a, c) in enumerate(zip(own_refs(4 * b + 1 - lo), stage_refs(b)))
+        ]
+
+    def onward_copies(d):
+        target = plane_peer(d)
+        return [
+            remote(a, c, w_send.at[k, planes + d], w_recv.at[k, planes + d], dev(target))
+            for k, (a, c) in enumerate(zip(stage_refs((hi + d) % 2), weight_refs(x_peer)))
+        ]
+
+    def stage_forward():
+        return [
+            remote(a, c, wf_send.at[k, planes], wf_recv.at[k, planes], dev(y_peer))
+            for k, (a, c) in enumerate(zip(stage_refs(hi % 2), weight_refs(x_peer)))
+        ]
+
     def start(copies):
         for copy in copies:
             copy.start()
@@ -366,8 +400,9 @@
             copy.wait_send()
 
     def relay_weights(i):
-        wait_recv(weight_copies(i))
-        start(forward_copies(i))
+        for arrived, onward in zip(weight_copies(i), forward_copies(i)):
+            arrived.wait_recv()
+            onward.start()
 
     for d in range(1, planes):
         start(z_copies(d))
@@ -417,11 +452,11 @@
 
     attend(0)
     lax.fori_loop(1, planes, first_step, 0)
+    start(stage_copies(0))
+    start(stage_copies(1))
     lax.fori_loop(1, planes, attend_step, 0)
     lax.fori_loop(0, planes, second_step, 0)
     start(own_forward())
-    for i in range(planes, 2 * planes):
-        start(weight_copies(i))
 
     def third_step(d, carry):
         first_copies(d)[3].wait_recv()
@@ -431,19 +466,26 @@
     def fourth_step(d, carry):
         first_copies(d)[2].wait_recv()
         attend(2 * planes + d)
+
+        @pl.when(d > 0)
+        def _():
+            relay_weights(d)
+
         return carry
 
     def fifth_step(d, carry):
         wait_recv(second_copies(d))
         attend(3 * planes + d)
-
-        @pl.when(d > 0)
-        def _():
-            relay_weights(d)
-
         return carry
 
     lax.fori_loop(0, planes, third_step, 0)
+    wait_recv(stage_copies(0))
+    wait_recv(stage_copies(1))
+    for d in range(1, planes):
+        start(onward_copies(d))
+    start(stage_forward())
+    for a, b in zip(stage_refs(hi % 2), weight_refs(x_peer)):
+        b[...] = a[...]
     lax.fori_loop(0, planes, fourth_step, 0)
     lax.fori_loop(0, planes, fifth_step, 0)
     for h in range(heads):
@@ -486,25 +528,27 @@
         token_copy(r).start()
     sibling_copy(0).start()
 
-    def relay_step(i, carry):
-        relay_weights(i)
-        return carry
-
-    lax.fori_loop(planes, 2 * planes, relay_step, 0)
-    for r in range(1, MEMBERS):
-        token_copy(r).wait_recv()
-        sibling_copy(r).start()
-
-    def arrive_step(i, carry):
-        wait_recv(
-            [
-                remote(a, a, wf_send.at[k, i], wf_recv.at[k, i], dev(y_peer))
-                for k, a in enumerate(weight_refs(source_peer(i) + 2 - 4 * mid))
-            ]
-        )
-        return carry
-
-    lax.fori_loop(0, 2 * planes, arrive_step, 0)
+    def relay_step(d, carry):
+        relay_weights(planes + d)
+        return carry
+
+    lax.fori_loop(1, planes, relay_step, 0)
+
+    def arrivals(i):
+        return [
+            remote(a, a, wf_send.at[k, i], wf_recv.at[k, i], dev(y_peer))
+            for k, a in enumerate(weight_refs(source_peer(i) + 2 - 4 * mid))
+        ]
+
+    def arrive_gate_up(i, carry):
+        wait_recv(arrivals(i)[:2])
+        return carry
+
+    def arrive_down(i, carry):
+        arrivals(i)[2].wait_recv()
+        return carry
+
+    lax.fori_loop(0, 2 * planes, arrive_gate_up, 0)
 
     def half_copy(r):
         return remote(
@@ -516,28 +560,43 @@
             share_send.at[r], share_recv.at[r], o_send.at[1, r], o_recv.at[1, r], dev(member(r))
         )
 
-    def mix_step(step, carry):
-        r = (step + 1) % MEMBERS
+    def mix_rows(rows, tokens_half):
+        both = jnp.dot(tokens_half, gate_up[...], preferred_element_type=f32)
+        attended[rows, 0:part] = gated(both[:, :part], both[:, part:])
+
+    def finish(r):
+        half_copy(r).wait_recv()
+        share_send[r] = (share_own[r] + half_recv[r].astype(f32)).astype(bf16)
+
+    def mix_step(r, carry):
+        @pl.when(r > 0)
+        def _():
+            token_copy(r).wait_recv()
+            sibling_copy(r).start()
+
+        mix_rows(own_rows, tokens[r, t])
         sibling_arrival(r).wait_recv()
-        rows = tokens[r].reshape(2 * share, model)
-        both = jnp.dot(rows, gate_up[...], preferred_element_type=f32)
-        hidden = gated(both[:, :part], both[:, part:])
-        attended[:, 0:part] = hidden
+        mix_rows(other_rows, tokens[r, 1 - t])
+
+        @pl.when(r == 0)
+        def _():
+            lax.fori_loop(0, 2 * planes, arrive_down, 0)
+
         half_send[r] = jnp.dot(
             attended[other_rows, 0:part], down[...], preferred_element_type=f32
         ).astype(bf16)
         half_copy(r).start()
-        partial = jnp.dot(attended[own_rows, 0:part], down[...], preferred_element_type=f32)
-        half_copy(r).wait_recv()
-        share_send[r] = (partial + half_recv[r].astype(f32)).astype(bf16)
+        share_own[r] = jnp.dot(attended[own_rows, 0:part], down[...], preferred_element_type=f32)
 
         @pl.when(r > 0)
         def _():
+            finish(r)
             share_copy(r).start()
 
         return carry
 
     lax.fori_loop(0, MEMBERS, mix_step, 0)
+    finish(0)
     out = middle[...].astype(f32) + share_send[0].astype(f32)
     for r in range(1, MEMBERS):
         share_copy(r).wait_recv()
@@ -550,9 +609,14 @@
         wait_send(first_copies(d))
         wait_send(second_copies(d))
     wait_send(own_forward())
-    for i in range(1, 2 * planes):
-        wait_send(weight_copies(i))
-        wait_send(forward_copies(i))
+    for b in range(2):
+        wait_send(stage_copies(b))
+    wait_send(stage_forward())
+    for d in range(1, planes):
+        wait_send(weight_copies(d))
+        wait_send(onward_copies(d))
+        wait_send(forward_copies(d))
+        wait_send(forward_copies(planes + d))
     head_copy.wait_send()
     for r in range(MEMBERS):
         sibling_copy(r).wait_send()
@@ -572,7 +636,7 @@
     head_size = query_gain.shape[0]
     heads = width // head_size
     share, model = residual_in.shape
-    part = gate_weight.shape[1] // MEMBERS
+    depth, part = gate_weight.shape[0], gate_weight.shape[1] // MEMBERS
     f32, bf16 = jnp.float32, jnp.bfloat16
     cosine, sine = rotary_tables(tok_rows, head_size)
     vmem = pl.BlockSpec(memory_space=pltpu.VMEM)
@@ -597,16 +661,21 @@
             pltpu.VMEM((MEMBERS, 2, share, model), bf16),
             pltpu.VMEM((model, 2 * part), bf16),
             pltpu.VMEM((part, model), bf16),
+            pltpu.VMEM((2, depth, 2 * part), bf16),
+            pltpu.VMEM((2, part, depth), bf16),
             pltpu.VMEM((MEMBERS, share, model), bf16),
             pltpu.VMEM((MEMBERS, share, model), bf16),
             pltpu.VMEM((MEMBERS, share, model), bf16),
             pltpu.VMEM((MEMBERS, share, model), bf16),
+            pltpu.VMEM((MEMBERS, share, model), f32),
             dma((2, 3, n_sp)),
             dma((2, n_sp)),
             dma((3, 2 * planes)),
             dma((3, 2 * planes)),
             dma((3, 2 * planes)),
             dma((3, 2 * planes)),
+            dma((3, 2)),
+            dma((3, 2)),
             dma,
             dma,
             dma((2, MEMBERS)),

time: 139 us -> 130 us (0.935)
  Pallas kernels: 136 us -> 127 us
    pallas_call x1, Pallas kernels: 136 us -> 127 us  [fused(): pl.pallas_call(functools.partial(layer_kernel, n_sp), out_shape=jax.Shape...]
where the time goes in v2:
time: 130 us
  Pallas kernels  127 us (98%)
  local copies, waits for them, and re-layouts  1.88 us (1%)
    pallas_call x1, Pallas kernels, fused(): pl.pallas_call(functools.partial(layer_kernel, n_sp), out_shape=jax.Shape...  127 us

profile of v2, /device:TPU:0, one launch (start us, length us, event | category | flops | bytes accessed | tf_op | source)
XLA Modules:
  0.0 130.3 jit_solution(14131328133142317893)
XLA Ops:
  0.0 1.3 sine_multiply_fusion
  1.3 127.2 %shard_map.109 = bf16[128,2048]{1,0:T(8,128)(2,1)} custom-call(bf16[256,512]{1,0:T(8,128)(2,1)} %queries.1, bf16[256,256]{1,0:T(8,128)(2,1)} %keys.1, bf16[256,256]{1,0:T(8,128)(2,1)} %values.1, f32[1,128]{1,0:T(1,128)} %bitcast.4, f32[1,128]{1,0:T(1,128)} %bitcast.5, bf16[128,2048]{1,0:T(8,128)(2,1)} %residual_in.1, bf16[512,2048]{1,0:T(8,128)(2,1)} %out_weight.1, ...), custom_call_target="tpu_custom_call" | custom-call | tf_op jit(solution)/shard_map/pallas_call | solution.py:644
  128.4 1.9 %copy.13 = bf16[128,2048]{1,0:T(8,128)(2,1)} copy(bf16[128,2048]{1,0:T(8,128)(2,1)} %shard_map.109) | data formatting | bytes 1048576
  (3 shorter events, 0.0 us)
